TPU v7x, 32 devices: a whole 2x2x4 slice. The times are simulated.
32 devices in a mesh: fs: 16 (over z, y, x), tp: 2 (over core).
Axes of the slice: x: 2, y: 2, z: 4, core: 2. Of those that a mesh axis runs over, the one named last changes fastest.
Arguments:
- tokens: bfloat16 [2, 256, 2048], P('tp'), may hold values from -6 to 6
- gain_first: float32 [2048], P('fs'), may hold values from 0.1 to 1.9
- gate_first: float32 [2048, 5632], P('fs', 'tp'), may hold values from -0.125 to 0.125
- up_first: float32 [2048, 5632], P('fs', 'tp'), may hold values from -0.125 to 0.125
- down_first: float32 [2048, 5632], P('fs', 'tp'), may hold values from -0.3125 to 0.3125
- gain_second: float32 [2048], P('fs'), may hold values from 0.1 to 1.9
- gate_second: float32 [2048, 5632], P('fs', 'tp'), may hold values from -0.125 to 0.125
- up_second: float32 [2048, 5632], P('fs', 'tp'), may hold values from -0.125 to 0.125
- down_second: float32 [2048, 5632], P('fs', 'tp'), may hold values from -0.3125 to 0.3125
Outputs:
- mixed: bfloat16 [2, 256, 2048], P('tp', 'fs')
- served_gate_first: bfloat16 [2, 2816, 2048], P(None, 'fs')
- served_up_first: bfloat16 [2, 2816, 2048], P(None, 'fs')
- served_down_first: bfloat16 [2, 2816, 2048], P(None, 'fs')
- served_gate_second: bfloat16 [2, 2816, 2048], P(None, 'fs')
- served_up_second: bfloat16 [2, 2816, 2048], P(None, 'fs')
- served_down_second: bfloat16 [2, 2816, 2048], P(None, 'fs')
All inputs are finite; a program needn't handle non-finite values.
Results may differ from a plain program's by a relative error of at most 0.013.
Values may be sent and summed in bfloat16 or wider, within the bound.
A program may use at most 64 MiB of HBM per device.

v0:
```python
import jax
import jax.numpy as jnp
from jax import lax
from jax.sharding import PartitionSpec as P


def normalize(values):
    wide = values.astype(jnp.float32)
    scale = lax.rsqrt(jnp.mean(wide * wide, axis=-1, keepdims=True) + 1e-06)
    return (wide * scale).astype(jnp.bfloat16)


def folded(weight, gain):
    return (weight * gain[:, None]).astype(jnp.bfloat16).T


def relayout(gate_part, up_part, down_part):
    gate_cut, up_cut, down_cut = (
        lax.all_to_all(gate_part, "fs", split_axis=0, concat_axis=1, tiled=True),
        lax.all_to_all(up_part, "fs", split_axis=0, concat_axis=1, tiled=True),
        lax.all_to_all(down_part, "fs", split_axis=0, concat_axis=1, tiled=True),
    )
    return (
        lax.all_gather(gate_cut[None], "tp", axis=0, tiled=True),
        lax.all_gather(up_cut[None], "tp", axis=0, tiled=True),
        lax.all_gather(down_cut[None], "tp", axis=0, tiled=True),
    )


def hidden_of(normed, gate_served, up_served):
    gate_flat = gate_served.reshape(-1, gate_served.shape[2])
    up_flat = up_served.reshape(-1, up_served.shape[2])
    gate_act = jnp.einsum("rd,hd->rh", normed, gate_flat, preferred_element_type=jnp.float32)
    up_act = jnp.einsum("rd,hd->rh", normed, up_flat, preferred_element_type=jnp.float32)
    return (jax.nn.silu(gate_act) * up_act).astype(jnp.bfloat16)


def projector(hidden, down_flat):
    return jnp.dot(hidden, down_flat, preferred_element_type=jnp.float32)


def shards(
    tokens,
    gain_first,
    gate_first,
    up_first,
    down_first,
    gain_second,
    gate_second,
    up_second,
    down_second,
):
    gate_one, up_one, down_one = relayout(
        folded(gate_first, gain_first),
        folded(up_first, gain_first),
        down_first.astype(jnp.bfloat16).T,
    )
    gate_two, up_two, down_two = relayout(
        folded(gate_second, gain_second),
        folded(up_second, gain_second),
        down_second.astype(jnp.bfloat16).T,
    )
    rows = tokens[0]
    keep = rows.shape[0] // lax.axis_size("fs")
    offset = lax.axis_index("fs") * keep
    hidden_first = hidden_of(normalize(rows), gate_one, up_one)
    down_flat_one = down_one.reshape(-1, down_one.shape[2])
    partial_value = jnp.dot(hidden_first, down_flat_one, preferred_element_type=jnp.float32)
    branch = lax.psum(partial_value, "fs")
    whole_middle = (rows.astype(jnp.float32) + 0.5 * branch).astype(jnp.bfloat16)
    hidden_second = hidden_of(normalize(whole_middle), gate_two, up_two)
    middle = lax.dynamic_slice_in_dim(whole_middle, offset, keep, 0)
    down_flat_two = down_two.reshape(-1, down_two.shape[2])
    branch_two = lax.psum_scatter(
        projector(hidden_second, down_flat_two), "fs", scatter_dimension=0, tiled=True
    )
    mixed = (middle.astype(jnp.float32) + 0.5 * branch_two).astype(jnp.bfloat16)[None]
    return (mixed, gate_one, up_one, down_one, gate_two, up_two, down_two)


def solution(mesh):
    return jax.shard_map(
        shards,
        mesh=mesh,
        in_specs=(
            P("tp", None, None),
            P("fs"),
            P("fs", "tp"),
            P("fs", "tp"),
            P("fs", "tp"),
            P("fs"),
            P("fs", "tp"),
            P("fs", "tp"),
            P("fs", "tp"),
        ),
        out_specs=(
            P("tp", "fs", None),
            P(None, "fs", None),
            P(None, "fs", None),
            P(None, "fs", None),
            P(None, "fs", None),
            P(None, "fs", None),
            P(None, "fs", None),
        ),
        check_vma=False,
    )
```

profile of v0, /device:TPU:0, one launch (start us, length us, event | category | flops | bytes accessed | tf_op | source)
XLA Modules:
  0.0 395.1 jit_solution(5311903597791260053)
XLA Ops:
  7.2 1.8 copy.40
  9.0 1.8 copy.42
  11.9 28.1 %all_to_all.96 = bf16[16,176,128]{2,1,0:T(8,128)(2,1)S(1)} all-to-all(bf16[16,176,128]{2,1,0:T(8,128)(2,1)S(1)} %bitcast.56), channel_id=1, replica_groups=mesh['fs'=16,'tp'=2] {'fs'}, dimensions={0} | all-to-all | bytes 1441792 | tf_op jit(solution)/shard_map/all_to_all | solution.py:19
  40.3 1.2 broadcast_in_dim.27
  41.5 22.3 %all_to_all.97 = bf16[16,176,128]{2,1,0:T(8,128)(2,1)S(1)} all-to-all(bf16[16,176,128]{2,1,0:T(8,128)(2,1)S(1)} %bitcast.54), channel_id=1, replica_groups=mesh['fs'=16,'tp'=2] {'fs'}, dimensions={0} | all-to-all | bytes 1441792 | tf_op jit(solution)/shard_map/all_to_all | solution.py:20
  64.0 1.2 broadcast_in_dim.28
  66.0 22.3 %all_to_all.98 = bf16[16,176,128]{2,1,0:T(8,128)(2,1)S(1)} all-to-all(bf16[16,176,128]{2,1,0:T(8,128)(2,1)S(1)} %bitcast.64), channel_id=1, replica_groups=mesh['fs'=16,'tp'=2] {'fs'}, dimensions={0} | all-to-all | bytes 1441792 | tf_op jit(solution)/shard_map/all_to_all | solution.py:21
  88.5 1.2 broadcast_in_dim.29
  90.6 1.8 copy.48
  92.4 1.6 fusion.4
  94.0 2.5 fusion.14
  97.1 5.5 %fusion.10 = f32[256,2048]{1,0:T(8,128)} fusion(bf16[352,2048]{1,0:T(8,128)(2,1)} %bitcast.68, bf16[352,2048]{1,0:T(8,128)(2,1)} %bitcast.67, bf16[1,256,2048]{2,1,0:T(8,128)(2,1)} %param.9, f32[256]{0:T(256)S(1)} %add_rsqrt_fusion.1, f32[256,352]{0,1:T(8,128)S(1)} %fusion.14), kind=kOutput, calls=%fused_computation.20 | convolution fusion | flops 740311040 | bytes 6390784 | tf_op jit(solution)/shard_map/dot_general | solution.py:68
  104.3 41.4 %all_to_all.99 = bf16[16,176,128]{2,1,0:T(8,128)(2,1)S(1)} all-to-all(bf16[16,176,128]{2,1,0:T(8,128)(2,1)S(1)} %bitcast.57), channel_id=1, replica_groups=mesh['fs'=16,'tp'=2] {'fs'}, dimensions={0} | all-to-all | bytes 1441792 | tf_op jit(solution)/shard_map/all_to_all | solution.py:19
  147.2 26.7 %all_to_all.100 = bf16[16,176,128]{2,1,0:T(8,128)(2,1)S(1)} all-to-all(bf16[16,176,128]{2,1,0:T(8,128)(2,1)S(1)} %bitcast.55), channel_id=1, replica_groups=mesh['fs'=16,'tp'=2] {'fs'}, dimensions={0} | all-to-all | bytes 1441792 | tf_op jit(solution)/shard_map/all_to_all | solution.py:20
  176.0 23.5 %all_to_all.101 = bf16[16,176,128]{2,1,0:T(8,128)(2,1)S(1)} all-to-all(bf16[16,176,128]{2,1,0:T(8,128)(2,1)S(1)} %bitcast.65), channel_id=1, replica_groups=mesh['fs'=16,'tp'=2] {'fs'}, dimensions={0} | all-to-all | bytes 1441792 | tf_op jit(solution)/shard_map/all_to_all | solution.py:21
  201.2 50.3 %all-reduce.2.cloned.1.call-done = f32[256,2048]{1,0:T(8,128)} async-done(((f32[256,2048]{1,0:T(8,128)}), f32[256,2048]{1,0:T(8,128)}) %all-reduce.2.cloned.1.call-update) | async-done | bytes 2097168 | tf_op jit(solution)/shard_map/psum | solution.py:69
  251.4 2.1 fusion.2
  253.6 8.7 %all-gather.13.cloned.1.call-done = bf16[2,176,2048]{2,1,0:T(8,128)(2,1)} async-done(((bf16[1,176,2048]{2,1,0:T(8,128)(2,1)}), bf16[2,176,2048]{2,1,0:T(8,128)(2,1)}) %all-gather.13.cloned.1.call-update) | async-done | bytes 1441808 | tf_op jit(solution)/shard_map/all_gather | solution.py:24
  262.3 2.0 fusion.18
  264.3 10.8 %all-gather.15.cloned.1.call-done = bf16[2,176,2048]{2,1,0:T(8,128)(2,1)} async-done(((bf16[1,176,2048]{2,1,0:T(8,128)(2,1)}), bf16[2,176,2048]{2,1,0:T(8,128)(2,1)}) %all-gather.15.cloned.1.call-update) | async-done | bytes 1441808 | tf_op jit(solution)/shard_map/all_gather | solution.py:25
  275.1 12.9 %all-gather.17.cloned.1.call-done = bf16[2,176,2048]{2,1,0:T(8,128)(2,1)} async-done(((bf16[1,176,2048]{2,1,0:T(8,128)(2,1)}), bf16[2,176,2048]{2,1,0:T(8,128)(2,1)}) %all-gather.17.cloned.1.call-update) | async-done | bytes 1441808 | tf_op jit(solution)/shard_map/all_gather | solution.py:26
  288.0 5.2 %fusion.9 = f32[256,2048]{1,0:T(8,128)} fusion(bf16[352,2048]{1,0:T(8,128)(2,1)} %bitcast.71, bf16[352,2048]{1,0:T(8,128)(2,1)} %bitcast.70, bf16[256,2048]{1,0:T(8,128)(2,1)S(1)} %get-tuple-element.8, f32[256]{0:T(256)S(1)} %add_rsqrt_fusion, f32[256,352]{0,1:T(8,128)S(1)} %fusion.18), kind=kOutput, calls=%fused_computation.19 | convolution fusion | flops 740311040 | bytes 6390784 | tf_op jit(solution)/shard_map/dot_general | solution.py:39
  293.3 82.9 %reduce-scatter.2.cloned.1.call-done = f32[16,2048]{1,0:T(8,128)} async-done(((f32[256,2048]{1,0:T(8,128)}), f32[16,2048]{1,0:T(8,128)}) %reduce-scatter.2.cloned.1.call-update) | async-done | bytes 131088 | tf_op jit(solution)/shard_map/reduce_scatter | solution.py:74
  376.2 1.6 fusion.32
  (69 shorter events, 21.4 us)
Async XLA Ops:
  7.2 86.8 %all-gather.7.cloned.1.call-start = ((), (), s32[]{:S(2)}) async-start(), calls=%async_computation.7 | async-start | bytes 2162688 | tf_op jit(solution)/shard_map/all_gather | solution.py:24
  9.0 1.8 copy-start.12
  40.2 1.3 copy-start.1
  41.4 55.1 %all-gather.9.cloned.1.call-start = ((), (), s32[]{:S(2)}) async-start(), calls=%async_computation.8 | async-start | bytes 2162688 | tf_op jit(solution)/shard_map/all_gather | solution.py:25
  64.0 1.6 copy-start.3
  65.2 31.9 %all-gather.11.cloned.1.call-start = ((), (), s32[]{:S(2)}) async-start(), calls=%async_computation.9 | async-start | bytes 2162688 | tf_op jit(solution)/shard_map/all_gather | solution.py:26
  88.5 1.6 copy-start.4
  89.7 161.7 %all-reduce.2.cloned.1.call-start = ((), (), s32[]{:S(2)}) async-start(), calls=%async_computation.10 | async-start | bytes 4194304 | tf_op jit(solution)/shard_map/psum | solution.py:69
  102.6 0.7 copy-start.13
  102.6 159.6 %all-gather.13.cloned.1.call-start = ((), (), s32[]{:S(2)}) async-start(), calls=%async_computation.11 | async-start | bytes 2162688 | tf_op jit(solution)/shard_map/all_gather | solution.py:24
  145.9 1.3 copy-start.2
  147.1 127.9 %all-gather.15.cloned.1.call-start = ((), (), s32[]{:S(2)}) async-start(), calls=%async_computation.12 | async-start | bytes 2162688 | tf_op jit(solution)/shard_map/all_gather | solution.py:25
  174.1 1.6 copy-start.5
  175.3 112.7 %all-gather.17.cloned.1.call-start = ((), (), s32[]{:S(2)}) async-start(), calls=%async_computation.13 | async-start | bytes 2162688 | tf_op jit(solution)/shard_map/all_gather | solution.py:26
  199.7 51.7 %copy-start = (bf16[1,256,2048]{2,1,0:T(8,128)(2,1)S(1)}, bf16[1,256,2048]{2,1,0:T(8,128)(2,1)}, u32[]{:S(2)}) copy-start(bf16[1,256,2048]{2,1,0:T(8,128)(2,1)} %param.9) | copy-start | bytes 3145732
  200.9 175.2 %reduce-scatter.2.cloned.1.call-start = ((), (), s32[]{:S(2)}) async-start(), calls=%async_computation.14 | async-start | bytes 2228224 | tf_op jit(solution)/shard_map/reduce_scatter | solution.py:74
  293.2 84.5 %copy-start.6 = (bf16[2,176,2048]{2,1,0:T(8,128)(2,1)S(1)}, bf16[2,176,2048]{2,1,0:T(8,128)(2,1)}, u32[]{:S(2)}) copy-start(bf16[2,176,2048]{2,1,0:T(8,128)(2,1)} %all-gather.7.cloned.1.call-done) | copy-start | bytes 4325380
  377.7 1.9 copy-start.7
  379.6 1.9 copy-start.8
  381.5 1.9 copy-start.9
  383.4 1.9 copy-start.10
  385.3 1.9 copy-start.11
Sparse Core Ops, SparseCore 0:
  41.6 7.2 all-gather.6
  65.3 7.2 all-gather.8
  89.8 7.2 all-gather.10
  102.8 148.6 all-reduce.1
  253.4 8.8 all-gather.12
  264.3 10.7 all-gather.14
  277.2 10.7 all-gather.16
  293.4 82.7 reduce-scatter.1
where the time goes:
time: 396 us; the launch traced here: 395 us
  waiting for transfers between devices  166 us (42%)
  blocking collectives  164 us (41%)
  local copies, waits for them, and re-layouts  26.9 us (7%)
  matrix products  15.3 us (4%)
  between operations  14.3 us (4%)
  other arithmetic  7.42 us (2%)
    reduce_scatter x1, waiting for transfers between devices, shards(): lax.psum_scatter(projector(hidden_second, down_flat_two), 'fs', scatter_d...  82.9 us
    all_to_all x2, blocking collectives, relayout(): lax.all_to_all(gate_part, 'fs', split_axis=0, concat_axis=1, tiled=True)  69.5 us
    psum x1, waiting for transfers between devices, shards(): branch = lax.psum(partial_value, 'fs')  50.3 us
    all_to_all x2, blocking collectives, relayout(): lax.all_to_all(up_part, 'fs', split_axis=0, concat_axis=1, tiled=True)  49 us
    all_to_all x2, blocking collectives, relayout(): lax.all_to_all(down_part, 'fs', split_axis=0, concat_axis=1, tiled=True)  45.8 us
    unnamed x40, local copies, waits for them, and re-layouts  18.8 us
    all_gather x2, waiting for transfers between devices, relayout(): lax.all_gather(down_cut[None], 'tp', axis=0, tiled=True)  13.5 us
    all_gather x2, waiting for transfers between devices, relayout(): lax.all_gather(up_cut[None], 'tp', axis=0, tiled=True)  10.8 us
  transfers between devices with their start and end apart: 8, of which 6 were waited for; matrix products, arithmetic and copies ran while one was open for 5% of the time, Pallas kernels for 0%

commit v1 on v0

--- a/solution.py
+++ b/solution.py
@@ -66,7 +66,7 @@
     hidden_first = hidden_of(normalize(rows), gate_one, up_one)
     down_flat_one = down_one.reshape(-1, down_one.shape[2])
     partial_value = jnp.dot(hidden_first, down_flat_one, preferred_element_type=jnp.float32)
-    branch = lax.psum(partial_value, "fs")
+    branch = jnp.sum(lax.all_gather(partial_value, "fs"), axis=0)
     whole_middle = (rows.astype(jnp.float32) + 0.5 * branch).astype(jnp.bfloat16)
     hidden_second = hidden_of(normalize(whole_middle), gate_two, up_two)
     middle = lax.dynamic_slice_in_dim(whole_middle, offset, keep, 0)

time: 396 us -> 641 us (1.62)
  waiting for transfers between devices: 166 us -> 365 us
  blocking collectives: 164 us -> 198 us
  other arithmetic: 7.42 us -> 19.6 us
    all_gather x0 -> x1, waiting for transfers between devices: none -> 259 us  [shards(): branch = jnp.sum(lax.all_gather(partial_value, 'fs'), axis=0)]
    psum x1 -> x0, waiting for transfers between devices: 50.3 us -> none  [shards(): branch = lax.psum(partial_value, 'fs')]
    all_to_all x2, blocking collectives: 45.8 us -> 63.9 us  [relayout(): lax.all_to_all(down_part, 'fs', split_axis=0, concat_axis=1, tiled=True)]
    reduce_sum x0 -> x1, other arithmetic: none -> 12.4 us  [shards(): branch = jnp.sum(lax.all_gather(partial_value, 'fs'), axis=0)]
    all_to_all x2, blocking collectives: 49 us -> 60.6 us  [relayout(): lax.all_to_all(up_part, 'fs', split_axis=0, concat_axis=1, tiled=True)]
    all_gather x2, waiting for transfers between devices: 8.75 us -> 0.02 us  [relayout(): lax.all_gather(gate_cut[None], 'tp', axis=0, tiled=True)]
    unnamed x40 -> x38, local copies, waits for them, and re-layouts: 18.8 us -> 20.3 us
  transfers between devices with their start and end apart: 8 -> 8, of which waited for: 6 -> 5; matrix products, arithmetic and copies ran while one was open for 5% -> 5% of each run, Pallas kernels for 0% -> 0%
where the time goes in v1:
time: 641 us
  waiting for transfers between devices  365 us (57%)
  blocking collectives  198 us (31%)
  local copies, waits for them, and re-layouts  28.4 us (4%)
  other arithmetic  19.6 us (3%)
  matrix products  14.7 us (2%)
  between operations  14.3 us (2%)
    all_gather x1, waiting for transfers between devices, shards(): branch = jnp.sum(lax.all_gather(partial_value, 'fs'), axis=0)  259 us
    reduce_scatter x1, waiting for transfers between devices, shards(): lax.psum_scatter(projector(hidden_second, down_flat_two), 'fs', scatter_d...  82.7 us
    all_to_all x2, blocking collectives, relayout(): lax.all_to_all(gate_part, 'fs', split_axis=0, concat_axis=1, tiled=True)  73.2 us
    all_to_all x2, blocking collectives, relayout(): lax.all_to_all(down_part, 'fs', split_axis=0, concat_axis=1, tiled=True)  63.9 us
    all_to_all x2, blocking collectives, relayout(): lax.all_to_all(up_part, 'fs', split_axis=0, concat_axis=1, tiled=True)  60.6 us
    unnamed x38, local copies, waits for them, and re-layouts  20.3 us
    all_gather x2, waiting for transfers between devices, relayout(): lax.all_gather(down_cut[None], 'tp', axis=0, tiled=True)  17.9 us
  transfers between devices with their start and end apart: 8, of which 5 were waited for; matrix products, arithmetic and copies ran while one was open for 5% of the time, Pallas kernels for 0%

profile of v1, /device:TPU:0, one launch (start us, length us, event | category | flops | bytes accessed | tf_op | source)
XLA Modules:
  0.0 640.5 jit_solution(450842090219323141)
XLA Ops:
  7.2 1.8 copy.40
  9.0 1.8 copy.42
  11.9 28.1 %all_to_all.96 = bf16[16,176,128]{2,1,0:T(8,128)(2,1)S(1)} all-to-all(bf16[16,176,128]{2,1,0:T(8,128)(2,1)S(1)} %bitcast.69), channel_id=1, replica_groups=mesh['fs'=16,'tp'=2] {'fs'}, dimensions={0} | all-to-all | bytes 1441792 | tf_op jit(solution)/shard_map/all_to_all | solution.py:19
  41.5 22.3 %all_to_all.97 = bf16[16,176,128]{2,1,0:T(8,128)(2,1)S(1)} all-to-all(bf16[16,176,128]{2,1,0:T(8,128)(2,1)S(1)} %bitcast.67), channel_id=1, replica_groups=mesh['fs'=16,'tp'=2] {'fs'}, dimensions={0} | all-to-all | bytes 1441792 | tf_op jit(solution)/shard_map/all_to_all | solution.py:20
  66.0 22.3 %all_to_all.98 = bf16[16,176,128]{2,1,0:T(8,128)(2,1)S(1)} all-to-all(bf16[16,176,128]{2,1,0:T(8,128)(2,1)S(1)} %bitcast.77), channel_id=1, replica_groups=mesh['fs'=16,'tp'=2] {'fs'}, dimensions={0} | all-to-all | bytes 1441792 | tf_op jit(solution)/shard_map/all_to_all | solution.py:21
  90.1 2.0 fusion.14
  92.1 4.9 all-gather.13.cloned.1.call-done
  97.1 5.2 fusion.9
  102.4 1.8 copy.46
  104.2 2.9 copy.48
  107.1 1.6 multiply_convert_fusion.2
  108.7 45.1 %all_to_all.99 = bf16[16,176,128]{2,1,0:T(8,128)(2,1)S(1)} all-to-all(bf16[16,176,128]{2,1,0:T(8,128)(2,1)S(1)} %bitcast.70), channel_id=1, replica_groups=mesh['fs'=16,'tp'=2] {'fs'}, dimensions={0} | all-to-all | bytes 1441792 | tf_op jit(solution)/shard_map/all_to_all | solution.py:19
  155.1 38.3 %all_to_all.100 = bf16[16,176,128]{2,1,0:T(8,128)(2,1)S(1)} all-to-all(bf16[16,176,128]{2,1,0:T(8,128)(2,1)S(1)} %bitcast.68), channel_id=1, replica_groups=mesh['fs'=16,'tp'=2] {'fs'}, dimensions={0} | all-to-all | bytes 1441792 | tf_op jit(solution)/shard_map/all_to_all | solution.py:20
  195.6 41.6 %all_to_all.101 = bf16[16,176,128]{2,1,0:T(8,128)(2,1)S(1)} all-to-all(bf16[16,176,128]{2,1,0:T(8,128)(2,1)S(1)} %bitcast.78), channel_id=1, replica_groups=mesh['fs'=16,'tp'=2] {'fs'}, dimensions={0} | all-to-all | bytes 1441792 | tf_op jit(solution)/shard_map/all_to_all | solution.py:21
  238.7 259.4 %all-gather.21.cloned.1.call-done = f32[4096,2048]{1,0:T(8,128)} async-done(((f32[256,2048]{1,0:T(8,128)}), f32[4096,2048]{1,0:T(8,128)}) %all-gather.21.cloned.1.call-update) | async-done | bytes 33554448 | tf_op jit(solution)/shard_map/all_gather | solution.py:69
  498.2 12.4 %reduce_sum.28 = f32[256,2048]{1,0:T(8,128)S(1)} reduce(f32[16,256,2048]{2,1,0:T(8,128)} %bitcast.63, f32[]{:T(128)} %constant.10.clone.1), dimensions={0}, to_apply=%region_1.2 | reduce | flops 7864320 | bytes 35651588 | tf_op jit(solution)/shard_map/reduce_sum | solution.py:69
  510.5 1.5 multiply_reduce_fusion
  512.0 1.3 fusion.10
  513.3 2.3 fusion.32
  515.6 5.1 all-gather.17.cloned.1.call-done
  520.7 12.9 %all-gather.19.cloned.1.call-done = bf16[2,176,2048]{2,1,0:T(8,128)(2,1)} async-done(((bf16[1,176,2048]{2,1,0:T(8,128)(2,1)}), bf16[2,176,2048]{2,1,0:T(8,128)(2,1)}) %all-gather.19.cloned.1.call-update) | async-done | bytes 1441808 | tf_op jit(solution)/shard_map/all_gather | solution.py:26
  533.7 5.2 fusion.8
  538.9 82.7 %reduce-scatter.2.cloned.1.call-done = f32[16,2048]{1,0:T(8,128)} async-done(((f32[256,2048]{1,0:T(8,128)}), f32[16,2048]{1,0:T(8,128)}) %reduce-scatter.2.cloned.1.call-update) | async-done | bytes 131088 | tf_op jit(solution)/shard_map/reduce_scatter | solution.py:74
  621.6 1.6 fusion.28
  (69 shorter events, 22.2 us)
Async XLA Ops:
  7.2 82.9 %all-gather.9.cloned.1.call-start = ((), (), s32[]{:S(2)}) async-start(), calls=%async_computation.7 | async-start | bytes 2162688 | tf_op jit(solution)/shard_map/all_gather | solution.py:24
  9.0 1.8 copy-start.11
  40.2 1.3 copy-start.5
  41.4 50.7 %all-gather.11.cloned.1.call-start = ((), (), s32[]{:S(2)}) async-start(), calls=%async_computation.8 | async-start | bytes 2162688 | tf_op jit(solution)/shard_map/all_gather | solution.py:25
  64.0 1.6 copy-start.6
  65.2 31.9 %all-gather.13.cloned.1.call-start = ((), (), s32[]{:S(2)}) async-start(), calls=%async_computation.9 | async-start | bytes 2162688 | tf_op jit(solution)/shard_map/all_gather | solution.py:26
  88.5 1.3 copy-start
  89.7 408.4 %all-gather.21.cloned.1.call-start = ((), (), s32[]{:S(2)}) async-start(), calls=%async_computation.14 | async-start | bytes 35651584 | tf_op jit(solution)/shard_map/all_gather | solution.py:69
  102.3 411.0 %all-gather.15.cloned.1.call-start = ((), (), s32[]{:S(2)}) async-start(), calls=%async_computation.10 | async-start | bytes 2162688 | tf_op jit(solution)/shard_map/all_gather | solution.py:24
  104.2 2.9 copy-start.12
  155.1 365.6 %all-gather.17.cloned.1.call-start = ((), (), s32[]{:S(2)}) async-start(), calls=%async_computation.11 | async-start | bytes 2162688 | tf_op jit(solution)/shard_map/all_gather | solution.py:25
  193.6 1.6 copy-start.7
  194.8 338.9 %all-gather.19.cloned.1.call-start = ((), (), s32[]{:S(2)}) async-start(), calls=%async_computation.12 | async-start | bytes 2162688 | tf_op jit(solution)/shard_map/all_gather | solution.py:26
  238.5 383.1 %reduce-scatter.2.cloned.1.call-start = ((), (), s32[]{:S(2)}) async-start(), calls=%async_computation.13 | async-start | bytes 2228224 | tf_op jit(solution)/shard_map/reduce_scatter | solution.py:74
  513.3 20.4 %copy-start.1 = (bf16[256,2048]{1,0:T(8,128)(2,1)S(1)}, bf16[256,2048]{1,0:T(8,128)(2,1)}, u32[]{:S(2)}) copy-start(bf16[256,2048]{1,0:T(8,128)(2,1)} %fusion.10) | copy-start | bytes 3145732
  538.8 84.3 %copy-start.8 = (bf16[2,176,2048]{2,1,0:T(8,128)(2,1)S(1)}, bf16[2,176,2048]{2,1,0:T(8,128)(2,1)}, u32[]{:S(2)}) copy-start(bf16[2,176,2048]{2,1,0:T(8,128)(2,1)} %all-gather.9.cloned.1.call-done) | copy-start | bytes 4325380
  623.2 1.9 copy-start.9
  625.0 1.9 copy-start.10
  626.9 1.9 copy-start.2
  628.8 1.9 copy-start.3
  630.7 1.9 copy-start.4
Sparse Core Ops, SparseCore 0:
  41.6 7.2 all-gather.8
  65.3 7.2 all-gather.10
  89.8 7.2 all-gather.12
  102.4 395.6 all-gather.20
  500.1 7.7 all-gather.14
  509.9 10.7 all-gather.16
  522.9 10.7 all-gather.18
  539.0 82.5 reduce-scatter.1
